TPU v7x, 32 devices: a whole 2x2x4 slice. The times are simulated.
32 devices in a mesh: ep: 8 (over z, core), tp: 4 (over y, x).
Axes of the slice: x: 2, y: 2, z: 4, core: 2. Of those that a mesh axis runs over, the one named last changes fastest.
Arguments:
- tokens: bfloat16 [1024, 2048], P('ep'), may hold values from -6 to 6
- selected: int32 [8, 256], P(None, 'ep'), may hold values from -1 to 127, as said below
- affinity: float32 [8, 256], P(None, 'ep'), may hold values from 0.05 to 1
- w_gate: bfloat16 [8, 2048, 2048], P('ep', None, 'tp'), may hold values from -0.125 to 0.125
- w_up: bfloat16 [8, 2048, 2048], P('ep', None, 'tp'), may hold values from -0.125 to 0.125
- w_down: bfloat16 [8, 2048, 2048], P('ep', 'tp'), may hold values from -0.125 to 0.125
Outputs:
- combined: bfloat16 [1024, 2048], P('ep', 'tp')
Inputs may be any that keep to these rules, and one draw needn't show every extreme that they name: `selected`: row e holds 8 aligned groups of 32 entries; the live entries of group j are distinct positions within the j-th block of 128 tokens, stand at the front of the group and are followed by -1; each row has 128 live entries in all, the number in a group varies, and some group of every row is full.
All inputs are finite; a program needn't handle non-finite values.
Results may differ from a plain program's by a relative error of at most 0.015.
Values may be sent and summed in bfloat16 or wider, within the bound.
A program may use at most 64 MiB of HBM per device.

v0:
```python
import functools
import math

import jax
import jax.numpy as jnp
from jax import lax
from jax.experimental import pallas as pl
from jax.experimental.pallas import tpu as pltpu
from jax.sharding import PartitionSpec as P

MESH = pl.DeviceIdType.MESH
F32 = jnp.float32
BF16 = jnp.bfloat16
CHUNK = 128
LAG = 2


def side_of(n):
    s = math.isqrt(n)
    while n % s:
        s -= 1
    return s


def kernel(
    n_ep, n_tp, chunks,
    tok_hbm, sel_hbm, aff_hbm, wg_hbm, wu_hbm, wd_hbm, out_ref,
    tok, sel, aff, wgu, wd, onehot, weight_hi, weight_lo, expand, compact,
    cnt_out, cnt_in, z_out, z_in, rows, acc, hid, part_out, part_in, ret_out, ret_in,
    s_in, s_w, s_cnt_s, s_cnt_r, s_z_s, s_z_r, s_x_s, s_x_r,
    s_p_s, s_p_r, s_r_s, s_r_r,
):
    ep = lax.axis_index("ep")
    tp = lax.axis_index("tp")
    n_tok, feats = tok.shape
    n_exp, group = sel.shape
    fc = feats // chunks
    live = rows.shape[2]
    hidden = hid.shape[1]

    width = side_of(n_tp)
    height = n_tp // width
    y, x = tp // width, lax.rem(tp, width)
    offsets = [(dy, dx) for dy in range(height) for dx in range(width)][1:]
    near = sorted(offsets, key=lambda o: (o[0] > 0) + (o[1] > 0))
    far = near[::-1]

    def tp_to(o):
        return lax.rem(y + o[0], height) * width + lax.rem(x + o[1], width)

    def tp_from(o):
        return lax.rem(y + height - o[0], height) * width + lax.rem(x + width - o[1], width)

    def tp_sem(o):
        return o[0] * width + o[1]

    ep_order = list(range(n_ep - 1))
    high_half = ep // (n_ep // 2)

    def ep_to(i):
        down = n_ep - 1 - i
        down = down - jnp.where(down <= ep, 1, 0)
        up = i + jnp.where(i >= ep, 1, 0)
        return jnp.where(high_half > 0, up, down)

    def rows_of(i):
        return pl.ds(pl.multiple_of(i * group, group), group)

    def cols(k, c):
        return pl.ds(pl.multiple_of(k * feats + c * fc, 128), fc)

    load_sel = pltpu.make_async_copy(sel_hbm, sel, s_in.at[0])
    load_tok = pltpu.make_async_copy(
        tok_hbm.at[:, pl.ds(pl.multiple_of(tp * feats, 128), feats)], tok, s_in.at[1]
    )
    load_aff = pltpu.make_async_copy(aff_hbm, aff, s_in.at[2])
    load_sel.start()
    load_tok.start()

    barrier = pltpu.get_barrier_semaphore()
    for d in ep_order:
        pl.semaphore_signal(barrier, inc=1, device_id={"ep": ep_to(d)}, device_id_type=MESH)
    for o in far:
        pl.semaphore_signal(barrier, inc=1, device_id={"tp": tp_to(o)}, device_id_type=MESH)

    load_aff.start()

    load_sel.wait()
    picked = sel[...].astype(F32)
    count = jnp.sum(jnp.where(picked >= 0, 1.0, 0.0), axis=1, keepdims=True)
    for e in range(n_exp):
        cnt_out[e] = jnp.broadcast_to(count[e:e + 1, :], (1, 128))
    picked_t = jnp.transpose(picked)
    token_lane = lax.broadcasted_iota(jnp.int32, (group, n_tok), 1).astype(F32)
    for e in range(n_exp):
        onehot[pl.ds(e * group, group), :] = jnp.where(
            picked_t[:, e:e + 1] == token_lane, 1.0, 0.0)
    load_tok.wait()
    pick = onehot[...].astype(BF16)
    for c in range(chunks):
        z_out[c] = jnp.dot(
            pick, tok[:, c * fc:(c + 1) * fc], preferred_element_type=F32).astype(BF16)
        z_in[c, rows_of(ep), :] = z_out[c, rows_of(ep), :]
    cnt_in[ep] = cnt_out[ep]

    pl.semaphore_wait(barrier, len(ep_order) + len(far))


    def send(src, dst, ss, rs, to):
        copy = pltpu.make_async_remote_copy(
            src_ref=src, dst_ref=dst, send_sem=ss, recv_sem=rs,
            device_id=to, device_id_type=MESH)
        copy.start()
        return copy

    others = (n_ep - 1) * group

    def whole(ref, ss, rs):
        return pltpu.make_async_remote_copy(
            src_ref=ref, dst_ref=ref, send_sem=ss, recv_sem=rs,
            device_id={"ep": ep_to(0)}, device_id_type=MESH)

    cnt_all = whole(cnt_in.at[pl.ds(0, n_ep - 1)], s_cnt_s.at[0], s_cnt_r.at[0])
    z_all = [
        whole(z_in.at[c, pl.ds(0, others), :], s_z_s.at[c], s_z_r.at[c]) for c in range(chunks)]
    r_all = [
        whole(ret_in.at[c, pl.ds(0, others), :], s_r_s.at[c], s_r_r.at[c]) for c in range(chunks)]

    for c in range(chunks):
        for d in ep_order:
            send(
                z_out.at[c, rows_of(ep_to(d)), :], z_in.at[c, rows_of(ep), :],
                s_z_s.at[c], s_z_r.at[c], {"ep": ep_to(d)})
            if c == 0:
                send(
                    cnt_out.at[ep_to(d)], cnt_in.at[ep],
                    s_cnt_s.at[0], s_cnt_r.at[0], {"ep": ep_to(d)})

    load_w = [
        pltpu.make_async_copy(wg_hbm.at[0], wgu.at[:, pl.ds(0, hidden)], s_w.at[0]),
        pltpu.make_async_copy(wu_hbm.at[0], wgu.at[:, pl.ds(hidden, hidden)], s_w.at[1]),
    ]
    load_d = [pltpu.make_async_copy(wd_hbm.at[0], wd, s_w.at[2])]
    for copy in load_w + load_d:
        copy.start()

    load_aff.wait()
    aff_t = jnp.transpose(aff[...])
    for e in range(n_exp):
        at = pl.ds(e * group, group)
        onehot[at, :] = onehot[at, :] * aff_t[:, e:e + 1]
    weight = jnp.transpose(onehot[...])
    high = weight.astype(BF16)
    weight_hi[...] = high
    weight_lo[...] = (weight - high.astype(F32)).astype(BF16)

    for copy in load_w:
        copy.wait()

    cnt_all.wait_recv()
    lane = lax.broadcasted_iota(jnp.int32, (group, live), 1).astype(F32)
    row = lax.broadcasted_iota(jnp.int32, (group, live), 0).astype(F32)
    start = jnp.zeros((group, live), F32)
    pieces = []
    for j in range(n_ep):
        n = jnp.broadcast_to(cnt_in[j, 0:1, 0:1], (group, live))
        pieces.append(jnp.where((lane - row == start) & (row < n), 1.0, 0.0))
        start = start + n
    spread = jnp.concatenate(pieces, axis=0)
    expand[...] = spread.astype(BF16)
    compact[...] = jnp.transpose(spread).astype(BF16)

    acc[...] = jnp.zeros_like(acc)
    x_copy = {}

    def take(c, k):
        acc[...] += jnp.dot(rows[c, k], wgu[cols(k, c), :], preferred_element_type=F32)

    def arrivals(c):
        for o in near:
            x_copy[c, o].wait_recv()
            take(c, tp_from(o))

    for c in range(chunks):
        z_all[c].wait_recv()
        rows[c, tp] = jnp.dot(
            compact[...], z_in[c], preferred_element_type=F32).astype(BF16)
        for o in near:
            x_copy[c, o] = send(
                rows.at[c, tp], rows.at[c, tp],
                s_x_s.at[c, tp_sem(o)], s_x_r.at[c, tp_sem(o)], {"tp": tp_to(o)})
        take(c, tp)
        if c >= LAG:
            arrivals(c - LAG)
    for c in range(max(0, chunks - LAG), chunks):
        arrivals(c)

    gate = acc[:, :hidden]
    up = acc[:, hidden:]
    hid[...] = (gate / (1.0 + jnp.exp(-gate)) * up).astype(BF16)

    for copy in load_d:
        copy.wait()

    p_copy = {}
    for c in range(chunks):
        for o in near + [(0, 0)]:
            k = tp_to(o)
            part_out[c, k] = jnp.dot(
                hid[...], wd[:, cols(k, c)], preferred_element_type=F32
            ).astype(BF16)
            if o != (0, 0):
                p_copy[c, o] = send(
                    part_out.at[c, k], part_in.at[c, tp],
                    s_p_s.at[c, tp_sem(o)], s_p_r.at[c, tp_sem(o)], {"tp": k})

    for c in range(chunks):
        total = part_out[c, tp].astype(F32)
        for o in near:
            p_copy[c, o].wait_recv()
            total = total + part_in[c, tp_from(o)].astype(F32)
        ret_out[c] = jnp.dot(
            expand[...], total.astype(BF16), preferred_element_type=F32).astype(BF16)
        for d in ep_order:
            send(
                ret_out.at[c, rows_of(ep_to(d)), :], ret_in.at[c, rows_of(ep), :],
                s_r_s.at[c], s_r_r.at[c], {"ep": ep_to(d)})
        ret_in[c, rows_of(ep), :] = ret_out[c, rows_of(ep), :]

    for copy in [cnt_all] + z_all + list(x_copy.values()) + list(p_copy.values()):
        copy.wait_send()

    for c in range(chunks):
        r_all[c].wait_recv()
        back = ret_in[c]
        out_ref[:, c * fc:(c + 1) * fc] = (
            jnp.dot(weight_hi[...], back, preferred_element_type=F32)
            + jnp.dot(weight_lo[...], back, preferred_element_type=F32)
        ).astype(BF16)

    for copy in r_all:
        copy.wait_send()


def per_device(tokens, selected, affinity, w_gate, w_up, w_down):
    n_ep = lax.axis_size("ep")
    n_tp = lax.axis_size("tp")
    n_tok, width = tokens.shape
    n_exp, group = selected.shape
    hidden = w_gate.shape[2]
    assert w_gate.shape[0] == 1 and n_exp == n_ep
    feats = width // n_tp
    chunks = max(1, feats // CHUNK)
    fc = feats // chunks
    slots = n_ep * group
    live = slots // 2
    dma = pltpu.SemaphoreType.DMA
    any_spec = pl.BlockSpec(memory_space=pl.ANY)
    return pl.pallas_call(
        functools.partial(kernel, n_ep, n_tp, chunks),
        out_shape=pltpu.VMEM((n_tok, feats), BF16),
        in_specs=[any_spec] * 6,
        out_specs=pl.BlockSpec(memory_space=pltpu.VMEM),
        scratch_shapes=[
            pltpu.VMEM((n_tok, feats), BF16),
            pltpu.VMEM((n_exp, group), jnp.int32),
            pltpu.VMEM((n_exp, group), F32),
            pltpu.VMEM((width, 2 * hidden), BF16),
            pltpu.VMEM((hidden, width), BF16),
            pltpu.VMEM((slots, n_tok), F32),
            pltpu.VMEM((n_tok, slots), BF16),
            pltpu.VMEM((n_tok, slots), BF16),
            pltpu.VMEM((slots, live), BF16),
            pltpu.VMEM((live, slots), BF16),
            pltpu.VMEM((n_exp, 1, 128), F32),
            pltpu.VMEM((n_ep, 1, 128), F32),
            pltpu.VMEM((chunks, slots, fc), BF16),
            pltpu.VMEM((chunks, slots, fc), BF16),
            pltpu.VMEM((chunks, n_tp, live, fc), BF16),
            pltpu.VMEM((live, 2 * hidden), F32),
            pltpu.VMEM((live, hidden), BF16),
            pltpu.VMEM((chunks, n_tp, live, fc), BF16),
            pltpu.VMEM((chunks, n_tp, live, fc), BF16),
            pltpu.VMEM((chunks, slots, fc), BF16),
            pltpu.VMEM((chunks, slots, fc), BF16),
            dma((3,)),
            dma((3,)),
            dma((1,)),
            dma((1,)),
            dma((chunks,)),
            dma((chunks,)),
            dma((chunks, n_tp)),
            dma((chunks, n_tp)),
            dma((chunks, n_tp)),
            dma((chunks, n_tp)),
            dma((chunks,)),
            dma((chunks,)),
        ],
        compiler_params=pltpu.CompilerParams(collective_id=0, has_side_effects=True),
    )(tokens, selected, affinity, w_gate, w_up, w_down)


def solution(mesh):
    placed = (
        P("ep", None),
        P(None, "ep"),
        P(None, "ep"),
        P("ep", None, "tp"),
        P("ep", None, "tp"),
        P("ep", "tp", None),
    )
    return jax.shard_map(
        per_device, mesh=mesh, in_specs=placed, out_specs=P("ep", "tp"), check_vma=False
    )
```

profile of v0, /device:TPU:0, one launch (start us, length us, event | category | flops | bytes accessed | tf_op | source)
XLA Modules:
  0.0 31.1 jit_solution(14840333539742878817)
XLA Ops:
  0.0 30.4 %shard_map.64 = bf16[128,512]{1,0:T(8,128)(2,1)S(1)} custom-call(bf16[128,2048]{1,0:T(8,128)(2,1)} %tok_hbm.1, s32[8,32]{1,0:T(8,128)} %sel_hbm.1, f32[8,32]{1,0:T(8,128)} %aff_hbm.1, bf16[1,2048,512]{2,1,0:T(8,128)(2,1)} %wg_hbm.1, bf16[1,2048,512]{2,1,0:T(8,128)(2,1)} %wu_hbm.1, bf16[1,512,2048]{2,1,0:T(8,128)(2,1)} %wd_hbm.1), custom_call_target="tpu_custom_call" | custom-call | tf_op jit(solution)/shard_map/pallas_call | solution.py:259
  30.4 0.7 %copy.8 = bf16[128,512]{1,0:T(8,128)(2,1)} copy(bf16[128,512]{1,0:T(8,128)(2,1)S(1)} %shard_map.64) | data formatting | bytes 262144
where the time goes:
time: 31.3 us; the launch traced here: 31.1 us
  Pallas kernels  30.4 us (97%)
  local copies, waits for them, and re-layouts  0.66 us (2%)
    pallas_call x1, Pallas kernels, per_device(): pl.pallas_call(functools.partial(kernel, n_ep, n_tp, chunks), out_shape=p...  30.4 us
    unnamed x1, local copies, waits for them, and re-layouts  0.66 us

commit v1 on v0

v1 whole, which is shorter than its diff:
```python
import functools
import math

import jax
import jax.numpy as jnp
from jax import lax
from jax.experimental import pallas as pl
from jax.experimental.pallas import tpu as pltpu
from jax.sharding import PartitionSpec as P

MESH = pl.DeviceIdType.MESH
F32 = jnp.float32
BF16 = jnp.bfloat16
CHUNK = 128


def side_of(n):
    s = math.isqrt(n)
    while n % s:
        s -= 1
    return s


def plan(n_tp, chunks):
    width = side_of(n_tp)
    height = n_tp // width
    offsets = [(dy, dx) for dy in range(height) for dx in range(width)][1:]
    far = sorted(offsets, key=lambda o: -((o[0] > 0) + (o[1] > 0)))
    extra = list(range(chunks - chunks // 2, chunks)) if (height, width) == (2, 2) else []
    shared = [[o for o in far if not (c in extra and o == (1, 1))] for c in range(chunks)]
    return width, height, far, extra, shared


def kernel(
    n_ep, n_tp, chunks,
    tok_hbm, sel_hbm, aff_hbm, wg_hbm, wu_hbm, wd_hbm, out_ref,
    tok, sel, aff, wgu, wd, onehot, weight_hi, weight_lo, expand, compact,
    cnt_out, cnt_in, z_out, z_in, rows, acc, hid, part_out, part_in, ret_out, ret_in,
    s_in, s_cnt, s_z_r, s_x_r, s_p_r, s_r_r, s_out,
):
    ep = lax.axis_index("ep")
    tp = lax.axis_index("tp")
    n_tok = tok.shape[0]
    n_exp, group = sel.shape
    fc = z_in.shape[2]
    feats = fc * chunks
    live = rows.shape[1]
    hidden = hid.shape[1]
    width, height, far, extra, shared = plan(n_tp, chunks)
    y, x = tp // width, lax.rem(tp, width)

    def tp_to(o):
        return lax.rem(y + o[0], height) * width + lax.rem(x + o[1], width)

    def tp_from(o):
        return lax.rem(y + height - o[0], height) * width + lax.rem(x + width - o[1], width)

    ep_order = list(range(n_ep - 1))
    high_half = ep // (n_ep // 2)

    def ep_to(i):
        down = n_ep - 1 - i
        down = down - jnp.where(down <= ep, 1, 0)
        up = i + jnp.where(i >= ep, 1, 0)
        return jnp.where(high_half > 0, up, down)

    def rows_of(i):
        return pl.ds(pl.multiple_of(i * group, group), group)

    def cols(k, c):
        return pl.ds(pl.multiple_of(k * feats + c * fc, 128), fc)

    def at(c, k):
        return c * n_tp + k

    z_chunks = [(c, (0, 0)) for c in range(chunks)] + [(c, (1, 1)) for c in extra]

    load_sel = pltpu.make_async_copy(sel_hbm, sel, s_in.at[0])
    load_sel.start()
    pltpu.make_async_copy(
        tok_hbm.at[:, pl.ds(pl.multiple_of(tp * feats, 128), feats)],
        tok.at[:, pl.ds(0, feats)], s_in.at[1]).start()
    if extra:
        first = extra[0] * fc
        start = pl.multiple_of(tp_to((1, 1)) * feats + first, 128)
        pltpu.make_async_copy(
            tok_hbm.at[:, pl.ds(start, feats - first)],
            tok.at[:, pl.ds(feats, feats - first)], s_in.at[1]).start()
    load_tok = pltpu.make_async_copy(tok, tok, s_in.at[1])

    barrier = pltpu.get_barrier_semaphore()
    for d in ep_order:
        pl.semaphore_signal(barrier, inc=1, device_id={"ep": ep_to(d)}, device_id_type=MESH)
    for o in far:
        pl.semaphore_signal(barrier, inc=1, device_id={"tp": tp_to(o)}, device_id_type=MESH)

    load_aff = pltpu.make_async_copy(aff_hbm, aff, s_in.at[2])
    load_aff.start()

    load_sel.wait()
    picked = sel[...].astype(F32)
    count = jnp.sum(jnp.where(picked >= 0, 1.0, 0.0), axis=1, keepdims=True)
    for e in range(n_exp):
        cnt_out[e] = jnp.broadcast_to(count[e:e + 1, :], (1, 128))
    picked_t = jnp.transpose(picked)
    token_lane = lax.broadcasted_iota(jnp.int32, (group, n_tok), 1).astype(F32)
    for e in range(n_exp):
        onehot[pl.ds(e * group, group), :] = jnp.where(
            picked_t[:, e:e + 1] == token_lane, 1.0, 0.0)
    load_tok.wait()
    pick = onehot[...].astype(BF16)

    def gather(i):
        z_out[i] = jnp.dot(
            pick, tok[:, i * fc:(i + 1) * fc], preferred_element_type=F32).astype(BF16)
        z_in[i, rows_of(ep), :] = z_out[i, rows_of(ep), :]

    for i in range(len(z_chunks)):
        gather(i)
    cnt_in[ep] = cnt_out[ep]

    pl.semaphore_wait(barrier, len(ep_order) + len(far))

    def send(src, dst, ss, rs, to):
        copy = pltpu.make_async_remote_copy(
            src_ref=src, dst_ref=dst, send_sem=ss, recv_sem=rs,
            device_id=to, device_id_type=MESH)
        copy.start()
        return copy

    others = (n_ep - 1) * group

    def whole(ref, ss, rs):
        return pltpu.make_async_remote_copy(
            src_ref=ref, dst_ref=ref, send_sem=ss, recv_sem=rs,
            device_id={"ep": ep_to(0)}, device_id_type=MESH)

    cnt_all = whole(cnt_in.at[pl.ds(0, n_ep - 1)], s_cnt.at[0], s_cnt.at[1])

    for d in ep_order:
        send(cnt_out.at[ep_to(d)], cnt_in.at[ep], s_cnt.at[0], s_cnt.at[1], {"ep": ep_to(d)})
    for i in range(len(z_chunks)):
        for d in ep_order:
            send(
                z_out.at[i, rows_of(ep_to(d)), :], z_in.at[i, rows_of(ep), :],
                s_out.at[0], s_z_r.at[i], {"ep": ep_to(d)})

    pltpu.make_async_copy(wg_hbm.at[0], wgu.at[:, pl.ds(0, hidden)], s_in.at[3]).start()
    pltpu.make_async_copy(wu_hbm.at[0], wgu.at[:, pl.ds(hidden, hidden)], s_in.at[3]).start()
    load_w = pltpu.make_async_copy(wgu, wgu, s_in.at[3])
    places = far + [(0, 0)]
    for c in range(chunks):
        for n, o in enumerate(places):
            pltpu.make_async_copy(
                wd_hbm.at[0, :, cols(tp_to(o), c)],
                wd.at[c, :, pl.ds(n * fc, fc)], s_in.at[4]).start()
    load_d = pltpu.make_async_copy(wd, wd, s_in.at[4])

    load_aff.wait()
    aff_t = jnp.transpose(aff[...])
    for e in range(n_exp):
        block = pl.ds(e * group, group)
        onehot[block, :] = onehot[block, :] * aff_t[:, e:e + 1]
    weight = jnp.transpose(onehot[...])
    high = weight.astype(BF16)
    weight_hi[...] = high
    weight_lo[...] = (weight - high.astype(F32)).astype(BF16)

    load_w.wait()
    acc[...] = jnp.zeros_like(acc)

    cnt_all.wait_recv()
    lane = lax.broadcasted_iota(jnp.int32, (group, live), 1).astype(F32)
    row = lax.broadcasted_iota(jnp.int32, (group, live), 0).astype(F32)
    begin = jnp.zeros((group, live), F32)
    pieces = []
    for j in range(n_ep):
        n = jnp.broadcast_to(cnt_in[j, 0:1, 0:1], (group, live))
        pieces.append(jnp.where((lane - row == begin) & (row < n), 1.0, 0.0))
        begin = begin + n
    spread = jnp.concatenate(pieces, axis=0)
    expand[...] = spread.astype(BF16)
    compact[...] = jnp.transpose(spread).astype(BF16)

    def take(c, k):
        acc[...] += jnp.dot(rows[at(c, k)], wgu[cols(k, c), :], preferred_element_type=F32)

    def squeeze(i):
        c, o = z_chunks[i]
        whole(z_in.at[i, pl.ds(0, others), :], s_out.at[0], s_z_r.at[i]).wait_recv()
        rows[at(c, tp_to(o))] = jnp.dot(
            compact[...], z_in[i], preferred_element_type=F32).astype(BF16)

    def arrivals(c):
        whole(rows.at[pl.ds(0, len(shared[c]))], s_out.at[1], s_x_r.at[c]).wait_recv()
        for o in shared[c]:
            take(c, tp_from(o))

    for c in range(chunks):
        squeeze(c)
        for o in shared[c]:
            send(
                rows.at[at(c, tp)], rows.at[at(c, tp)],
                s_out.at[1], s_x_r.at[c], {"tp": tp_to(o)})
        take(c, tp)
    for c in range(chunks):
        if c in extra:
            squeeze(chunks + extra.index(c))
            take(c, tp_to((1, 1)))
        arrivals(c)

    gate = acc[:, :hidden]
    up = acc[:, hidden:]
    hid[...] = (gate / (1.0 + jnp.exp(-gate)) * up).astype(BF16)

    load_d.wait()
    step = max(1, 256 // fc)
    for c in range(chunks):
        for n in range(0, n_tp, step):
            some = places[n:n + step]
            value = jnp.dot(
                hid[...], wd[c, :, n * fc:(n + len(some)) * fc], preferred_element_type=F32
            ).astype(BF16)
            for m, o in enumerate(some):
                k = tp_to(o)
                part_out[at(c, k)] = value[:, m * fc:(m + 1) * fc]
                if o != (0, 0):
                    send(
                        part_out.at[at(c, k)], part_in.at[at(c, tp)],
                        s_out.at[2], s_p_r.at[c], {"tp": k})

    for c in range(chunks):
        total = part_out[at(c, tp)].astype(F32)
        whole(part_in.at[pl.ds(0, n_tp - 1)], s_out.at[2], s_p_r.at[c]).wait_recv()
        for o in far:
            total = total + part_in[at(c, tp_from(o))].astype(F32)
        ret_out[c] = jnp.dot(
            expand[...], total.astype(BF16), preferred_element_type=F32).astype(BF16)
        for d in ep_order:
            send(
                ret_out.at[c, rows_of(ep_to(d)), :], ret_in.at[c, rows_of(ep), :],
                s_out.at[3], s_r_r.at[c], {"ep": ep_to(d)})
        ret_in[c, rows_of(ep), :] = ret_out[c, rows_of(ep), :]

    cnt_all.wait_send()
    whole(z_in.at[:, pl.ds(0, others), :], s_out.at[0], s_z_r.at[0]).wait_send()
    n_x = sum(len(s) for s in shared)
    whole(rows.at[pl.ds(0, n_x)], s_out.at[1], s_x_r.at[0]).wait_send()
    whole(part_in.at[pl.ds(0, chunks * (n_tp - 1))], s_out.at[2], s_p_r.at[0]).wait_send()

    for c in range(chunks):
        whole(ret_in.at[c, pl.ds(0, others), :], s_out.at[3], s_r_r.at[c]).wait_recv()
        back = ret_in[c]
        out_ref[:, c * fc:(c + 1) * fc] = (
            jnp.dot(weight_hi[...], back, preferred_element_type=F32)
            + jnp.dot(weight_lo[...], back, preferred_element_type=F32)
        ).astype(BF16)

    whole(ret_in.at[:, pl.ds(0, others), :], s_out.at[3], s_r_r.at[0]).wait_send()


def per_device(tokens, selected, affinity, w_gate, w_up, w_down):
    n_ep = lax.axis_size("ep")
    n_tp = lax.axis_size("tp")
    n_tok, width = tokens.shape
    n_exp, group = selected.shape
    hidden = w_gate.shape[2]
    assert w_gate.shape[0] == 1 and n_exp == n_ep
    feats = width // n_tp
    chunks = max(1, feats // CHUNK)
    fc = feats // chunks
    n_z = chunks + len(plan(n_tp, chunks)[3])
    slots = n_ep * group
    live = slots // 2
    dma = pltpu.SemaphoreType.DMA
    any_spec = pl.BlockSpec(memory_space=pl.ANY)
    return pl.pallas_call(
        functools.partial(kernel, n_ep, n_tp, chunks),
        out_shape=pltpu.VMEM((n_tok, feats), BF16),
        in_specs=[any_spec] * 6,
        out_specs=pl.BlockSpec(memory_space=pltpu.VMEM),
        scratch_shapes=[
            pltpu.VMEM((n_tok, n_z * fc), BF16),
            pltpu.VMEM((n_exp, group), jnp.int32),
            pltpu.VMEM((n_exp, group), F32),
            pltpu.VMEM((width, 2 * hidden), BF16),
            pltpu.VMEM((chunks, hidden, n_tp * fc), BF16),
            pltpu.VMEM((slots, n_tok), F32),
            pltpu.VMEM((n_tok, slots), BF16),
            pltpu.VMEM((n_tok, slots), BF16),
            pltpu.VMEM((slots, live), BF16),
            pltpu.VMEM((live, slots), BF16),
            pltpu.VMEM((n_exp, 1, 128), F32),
            pltpu.VMEM((n_ep, 1, 128), F32),
            pltpu.VMEM((n_z, slots, fc), BF16),
            pltpu.VMEM((n_z, slots, fc), BF16),
            pltpu.VMEM((chunks * n_tp, live, fc), BF16),
            pltpu.VMEM((live, 2 * hidden), F32),
            pltpu.VMEM((live, hidden), BF16),
            pltpu.VMEM((chunks * n_tp, live, fc), BF16),
            pltpu.VMEM((chunks * n_tp, live, fc), BF16),
            pltpu.VMEM((chunks, slots, fc), BF16),
            pltpu.VMEM((chunks, slots, fc), BF16),
            dma((5,)),
            dma((2,)),
            dma((n_z,)),
            dma((chunks,)),
            dma((chunks,)),
            dma((chunks,)),
            dma((4,)),
        ],
        compiler_params=pltpu.CompilerParams(collective_id=0, has_side_effects=True),
    )(tokens, selected, affinity, w_gate, w_up, w_down)


def solution(mesh):
    placed = (
        P("ep", None),
        P(None, "ep"),
        P(None, "ep"),
        P("ep", None, "tp"),
        P("ep", None, "tp"),
        P("ep", "tp", None),
    )
    return jax.shard_map(
        per_device, mesh=mesh, in_specs=placed, out_specs=P("ep", "tp"), check_vma=False
    )
```

time: 31.3 us -> 30.6 us (0.978)
  Pallas kernels: 30.4 us -> 29.7 us
    pallas_call x1, Pallas kernels: 30.4 us -> 29.7 us  [per_device(): pl.pallas_call(functools.partial(kernel, n_ep, n_tp, chunks), out_shape=p...]
where the time goes in v1:
time: 30.6 us; the launch traced here: 30.4 us
  Pallas kernels  29.7 us (97%)
  local copies, waits for them, and re-layouts  0.66 us (2%)
    pallas_call x1, Pallas kernels, per_device(): pl.pallas_call(functools.partial(kernel, n_ep, n_tp, chunks), out_shape=p...  29.7 us
    unnamed x1, local copies, waits for them, and re-layouts  0.66 us

profile of v1, /device:TPU:0, one launch (start us, length us, event | category | flops | bytes accessed | tf_op | source)
XLA Modules:
  0.0 30.4 jit_solution(3641919667484200732)
XLA Ops:
  0.0 29.7 %shard_map.64 = bf16[128,512]{1,0:T(8,128)(2,1)S(1)} custom-call(bf16[128,2048]{1,0:T(8,128)(2,1)} %tok_hbm.1, s32[8,32]{1,0:T(8,128)} %sel_hbm.1, f32[8,32]{1,0:T(8,128)} %aff_hbm.1, bf16[1,2048,512]{2,1,0:T(8,128)(2,1)} %wg_hbm.1, bf16[1,2048,512]{2,1,0:T(8,128)(2,1)} %wu_hbm.1, bf16[1,512,2048]{2,1,0:T(8,128)(2,1)} %wd_hbm.1), custom_call_target="tpu_custom_call" | custom-call | tf_op jit(solution)/shard_map/pallas_call | solution.py:277
  29.8 0.7 %copy.8 = bf16[128,512]{1,0:T(8,128)(2,1)} copy(bf16[128,512]{1,0:T(8,128)(2,1)S(1)} %shard_map.64) | data formatting | bytes 262144

commit v2 on v1

--- a/solution.py
+++ b/solution.py
@@ -12,6 +12,8 @@
 F32 = jnp.float32
 BF16 = jnp.bfloat16
 CHUNK = 128
+EXTRA = 2
+LATE = {1: [4], 2: [5]}
 
 
 def side_of(n):
@@ -26,7 +28,7 @@
     height = n_tp // width
     offsets = [(dy, dx) for dy in range(height) for dx in range(width)][1:]
     far = sorted(offsets, key=lambda o: -((o[0] > 0) + (o[1] > 0)))
-    extra = list(range(chunks - chunks // 2, chunks)) if (height, width) == (2, 2) else []
+    extra = list(range(chunks - EXTRA, chunks)) if (height, width) == (2, 2) else []
     shared = [[o for o in far if not (c in extra and o == (1, 1))] for c in range(chunks)]
     return width, height, far, extra, shared
 
@@ -139,11 +141,14 @@
 
     for d in ep_order:
         send(cnt_out.at[ep_to(d)], cnt_in.at[ep], s_cnt.at[0], s_cnt.at[1], {"ep": ep_to(d)})
-    for i in range(len(z_chunks)):
+    def spread_out(i):
         for d in ep_order:
             send(
                 z_out.at[i, rows_of(ep_to(d)), :], z_in.at[i, rows_of(ep), :],
                 s_out.at[0], s_z_r.at[i], {"ep": ep_to(d)})
+
+    for i in range(chunks):
+        spread_out(i)
 
     pltpu.make_async_copy(wg_hbm.at[0], wgu.at[:, pl.ds(0, hidden)], s_in.at[3]).start()
     pltpu.make_async_copy(wu_hbm.at[0], wgu.at[:, pl.ds(hidden, hidden)], s_in.at[3]).start()
@@ -202,6 +207,9 @@
             send(
                 rows.at[at(c, tp)], rows.at[at(c, tp)],
                 s_out.at[1], s_x_r.at[c], {"tp": tp_to(o)})
+        for i in LATE.get(c, ()):
+            if i < len(z_chunks):
+                spread_out(i)
         take(c, tp)
     for c in range(chunks):
         if c in extra:

time: 30.6 us -> 30.1 us (0.984)
  Pallas kernels: 29.7 us -> 29.2 us
    pallas_call x1, Pallas kernels: 29.7 us -> 29.2 us  [per_device(): pl.pallas_call(functools.partial(kernel, n_ep, n_tp, chunks), out_shape=p...]
where the time goes in v2:
time: 30.1 us; the launch traced here: 29.9 us
  Pallas kernels  29.2 us (97%)
  local copies, waits for them, and re-layouts  0.66 us (2%)
    pallas_call x1, Pallas kernels, per_device(): pl.pallas_call(functools.partial(kernel, n_ep, n_tp, chunks), out_shape=p...  29.2 us
    unnamed x1, local copies, waits for them, and re-layouts  0.66 us

profile of v2, /device:TPU:0, one launch (start us, length us, event | category | flops | bytes accessed | tf_op | source)
XLA Modules:
  0.0 29.9 jit_solution(4822766529026064418)
XLA Ops:
  0.0 29.2 %shard_map.64 = bf16[128,512]{1,0:T(8,128)(2,1)S(1)} custom-call(bf16[128,2048]{1,0:T(8,128)(2,1)} %tok_hbm.1, s32[8,32]{1,0:T(8,128)} %sel_hbm.1, f32[8,32]{1,0:T(8,128)} %aff_hbm.1, bf16[1,2048,512]{2,1,0:T(8,128)(2,1)} %wg_hbm.1, bf16[1,2048,512]{2,1,0:T(8,128)(2,1)} %wu_hbm.1, bf16[1,512,2048]{2,1,0:T(8,128)(2,1)} %wd_hbm.1), custom_call_target="tpu_custom_call" | custom-call | tf_op jit(solution)/shard_map/pallas_call | solution.py:285
  29.2 0.7 %copy.8 = bf16[128,512]{1,0:T(8,128)(2,1)} copy(bf16[128,512]{1,0:T(8,128)(2,1)S(1)} %shard_map.64) | data formatting | bytes 262144

commit v3 on v1

--- a/solution.py
+++ b/solution.py
@@ -12,6 +12,9 @@
 F32 = jnp.float32
 BF16 = jnp.bfloat16
 CHUNK = 128
+OUT_EXTRA = 2
+RET_EXTRA = 2
+SIDE_AT = 2
 
 
 def side_of(n):
@@ -26,9 +29,21 @@
     height = n_tp // width
     offsets = [(dy, dx) for dy in range(height) for dx in range(width)][1:]
     far = sorted(offsets, key=lambda o: -((o[0] > 0) + (o[1] > 0)))
-    extra = list(range(chunks - chunks // 2, chunks)) if (height, width) == (2, 2) else []
+    square = (height, width) == (2, 2)
+    extra = list(range(chunks))[max(0, chunks - OUT_EXTRA):] if square and chunks > OUT_EXTRA else []
+    back = list(range(RET_EXTRA)) if square and chunks > RET_EXTRA else []
     shared = [[o for o in far if not (c in extra and o == (1, 1))] for c in range(chunks)]
-    return width, height, far, extra, shared
+    reduced = [[o for o in far if not (c in back and o == (1, 1))] for c in range(chunks)]
+    return width, height, far, extra, back, shared, reduced
+
+
+def pieces_of(far, back, reduced, chunks):
+    order = []
+    for c in range(chunks):
+        order += [(c, o) for o in reduced[c]]
+        if c == 0:
+            order += [(b, (1, 1)) for b in back]
+    return order + [(c, (0, 0)) for c in range(chunks)]
 
 
 def kernel(
@@ -36,7 +51,8 @@
     tok_hbm, sel_hbm, aff_hbm, wg_hbm, wu_hbm, wd_hbm, out_ref,
     tok, sel, aff, wgu, wd, onehot, weight_hi, weight_lo, expand, compact,
     cnt_out, cnt_in, z_out, z_in, rows, acc, hid, part_out, part_in, ret_out, ret_in,
-    s_in, s_cnt, s_z_r, s_x_r, s_p_r, s_r_r, s_out,
+    side_out, side_in,
+    s_in, s_cnt, s_z_r, s_x_r, s_p_r, s_r_r, s_side_r, s_out,
 ):
     ep = lax.axis_index("ep")
     tp = lax.axis_index("tp")
@@ -46,7 +62,7 @@
     feats = fc * chunks
     live = rows.shape[1]
     hidden = hid.shape[1]
-    width, height, far, extra, shared = plan(n_tp, chunks)
+    width, height, far, extra, back, shared, reduced = plan(n_tp, chunks)
     y, x = tp // width, lax.rem(tp, width)
 
     def tp_to(o):
@@ -115,8 +131,7 @@
             pick, tok[:, i * fc:(i + 1) * fc], preferred_element_type=F32).astype(BF16)
         z_in[i, rows_of(ep), :] = z_out[i, rows_of(ep), :]
 
-    for i in range(len(z_chunks)):
-        gather(i)
+    gather(0)
     cnt_in[ep] = cnt_out[ep]
 
     pl.semaphore_wait(barrier, len(ep_order) + len(far))
@@ -139,21 +154,25 @@
 
     for d in ep_order:
         send(cnt_out.at[ep_to(d)], cnt_in.at[ep], s_cnt.at[0], s_cnt.at[1], {"ep": ep_to(d)})
-    for i in range(len(z_chunks)):
+    def spread_out(i):
         for d in ep_order:
             send(
                 z_out.at[i, rows_of(ep_to(d)), :], z_in.at[i, rows_of(ep), :],
                 s_out.at[0], s_z_r.at[i], {"ep": ep_to(d)})
 
+    spread_out(0)
+    for i in range(1, chunks):
+        gather(i)
+        spread_out(i)
+
     pltpu.make_async_copy(wg_hbm.at[0], wgu.at[:, pl.ds(0, hidden)], s_in.at[3]).start()
     pltpu.make_async_copy(wu_hbm.at[0], wgu.at[:, pl.ds(hidden, hidden)], s_in.at[3]).start()
     load_w = pltpu.make_async_copy(wgu, wgu, s_in.at[3])
-    places = far + [(0, 0)]
-    for c in range(chunks):
-        for n, o in enumerate(places):
-            pltpu.make_async_copy(
-                wd_hbm.at[0, :, cols(tp_to(o), c)],
-                wd.at[c, :, pl.ds(n * fc, fc)], s_in.at[4]).start()
+    for i in range(chunks, len(z_chunks)):
+        gather(i)
+    for i, (c, o) in enumerate(pieces_of(far, back, reduced, chunks)):
+        pltpu.make_async_copy(
+            wd_hbm.at[0, :, cols(tp_to(o), c)], wd.at[:, pl.ds(i * fc, fc)], s_in.at[4]).start()
     load_d = pltpu.make_async_copy(wd, wd, s_in.at[4])
 
     load_aff.wait()
@@ -191,10 +210,8 @@
         rows[at(c, tp_to(o))] = jnp.dot(
             compact[...], z_in[i], preferred_element_type=F32).astype(BF16)
 
-    def arrivals(c):
+    def arrive(c):
         whole(rows.at[pl.ds(0, len(shared[c]))], s_out.at[1], s_x_r.at[c]).wait_recv()
-        for o in shared[c]:
-            take(c, tp_from(o))
 
     for c in range(chunks):
         squeeze(c)
@@ -202,60 +219,87 @@
             send(
                 rows.at[at(c, tp)], rows.at[at(c, tp)],
                 s_out.at[1], s_x_r.at[c], {"tp": tp_to(o)})
+        if 0 < c <= len(extra):
+            spread_out(chunks + c - 1)
         take(c, tp)
     for c in range(chunks):
         if c in extra:
             squeeze(chunks + extra.index(c))
             take(c, tp_to((1, 1)))
-        arrivals(c)
+        arrive(c)
+        for o in shared[c]:
+            take(c, tp_from(o))
 
     gate = acc[:, :hidden]
     up = acc[:, hidden:]
     hid[...] = (gate / (1.0 + jnp.exp(-gate)) * up).astype(BF16)
-
     load_d.wait()
+
+    def give(i, value):
+        ret_out[i] = jnp.dot(expand[...], value, preferred_element_type=F32).astype(BF16)
+        for d in ep_order:
+            send(
+                ret_out.at[i, rows_of(ep_to(d)), :], ret_in.at[i, rows_of(ep), :],
+                s_out.at[3], s_r_r.at[i], {"ep": ep_to(d)})
+        ret_in[i, rows_of(ep), :] = ret_out[i, rows_of(ep), :]
+
+    def combined(i):
+        whole(ret_in.at[i, pl.ds(0, others), :], s_out.at[3], s_r_r.at[i]).wait_recv()
+        value = ret_in[i]
+        return (
+            jnp.dot(weight_hi[...], value, preferred_element_type=F32)
+            + jnp.dot(weight_lo[...], value, preferred_element_type=F32))
+
+    order = pieces_of(far, back, reduced, chunks)
     step = max(1, 256 // fc)
-    for c in range(chunks):
-        for n in range(0, n_tp, step):
-            some = places[n:n + step]
-            value = jnp.dot(
-                hid[...], wd[c, :, n * fc:(n + len(some)) * fc], preferred_element_type=F32
-            ).astype(BF16)
-            for m, o in enumerate(some):
-                k = tp_to(o)
-                part_out[at(c, k)] = value[:, m * fc:(m + 1) * fc]
-                if o != (0, 0):
-                    send(
-                        part_out.at[at(c, k)], part_in.at[at(c, tp)],
-                        s_out.at[2], s_p_r.at[c], {"tp": k})
+    for i in range(0, len(order), step):
+        some = order[i:i + step]
+        value = jnp.dot(
+            hid[...], wd[:, i * fc:(i + len(some)) * fc], preferred_element_type=F32).astype(BF16)
+        for m, (c, o) in enumerate(some):
+            k = tp_to(o)
+            piece = value[:, m * fc:(m + 1) * fc]
+            if o in reduced[c]:
+                part_out[at(c, k)] = piece
+                send(
+                    part_out.at[at(c, k)], part_in.at[at(c, tp)],
+                    s_out.at[2], s_p_r.at[c], {"tp": k})
+            elif o == (0, 0):
+                part_out[at(c, tp)] = piece
+            else:
+                give(chunks + back.index(c), piece)
 
     for c in range(chunks):
         total = part_out[at(c, tp)].astype(F32)
-        whole(part_in.at[pl.ds(0, n_tp - 1)], s_out.at[2], s_p_r.at[c]).wait_recv()
-        for o in far:
+        whole(part_in.at[pl.ds(0, len(reduced[c]))], s_out.at[2], s_p_r.at[c]).wait_recv()
+        for o in reduced[c]:
             total = total + part_in[at(c, tp_from(o))].astype(F32)
-        ret_out[c] = jnp.dot(
-            expand[...], total.astype(BF16), preferred_element_type=F32).astype(BF16)
-        for d in ep_order:
-            send(
-                ret_out.at[c, rows_of(ep_to(d)), :], ret_in.at[c, rows_of(ep), :],
-                s_out.at[3], s_r_r.at[c], {"ep": ep_to(d)})
-        ret_in[c, rows_of(ep), :] = ret_out[c, rows_of(ep), :]
+        give(c, total.astype(BF16))
+        if c == min(SIDE_AT, chunks - 1):
+            for b in range(len(back)):
+                side_out[b] = combined(chunks + b).astype(BF16)
+                send(
+                    side_out.at[b], side_in.at[b],
+                    s_out.at[4], s_side_r.at[b], {"tp": tp_to((1, 1))})
 
     cnt_all.wait_send()
     whole(z_in.at[:, pl.ds(0, others), :], s_out.at[0], s_z_r.at[0]).wait_send()
-    n_x = sum(len(s) for s in shared)
+    n_x = sum(len(offsets) for offsets in shared)
     whole(rows.at[pl.ds(0, n_x)], s_out.at[1], s_x_r.at[0]).wait_send()
-    whole(part_in.at[pl.ds(0, chunks * (n_tp - 1))], s_out.at[2], s_p_r.at[0]).wait_send()
-
-    for c in range(chunks):
-        whole(ret_in.at[c, pl.ds(0, others), :], s_out.at[3], s_r_r.at[c]).wait_recv()
-        back = ret_in[c]
-        out_ref[:, c * fc:(c + 1) * fc] = (
-            jnp.dot(weight_hi[...], back, preferred_element_type=F32)
-            + jnp.dot(weight_lo[...], back, preferred_element_type=F32)
-        ).astype(BF16)
-
+    n_p = sum(len(offsets) for offsets in reduced)
+    whole(part_in.at[pl.ds(0, n_p)], s_out.at[2], s_p_r.at[0]).wait_send()
+
+    plain = [c for c in range(chunks) if c not in back]
+    for c in plain[:1] + back + plain[1:]:
+        value = combined(c)
+        if c in back:
+            b = back.index(c)
+            whole(side_in.at[b], s_out.at[4], s_side_r.at[b]).wait_recv()
+            value = value + side_in[b].astype(F32)
+        out_ref[:, c * fc:(c + 1) * fc] = value.astype(BF16)
+
+    if back:
+        whole(side_in, s_out.at[4], s_side_r.at[0]).wait_send()
     whole(ret_in.at[:, pl.ds(0, others), :], s_out.at[3], s_r_r.at[0]).wait_send()
 
 
@@ -270,6 +314,9 @@
     chunks = max(1, feats // CHUNK)
     fc = feats // chunks
     n_z = chunks + len(plan(n_tp, chunks)[3])
+    n_back = len(plan(n_tp, chunks)[4])
+    n_ret = chunks + n_back
+    n_side = max(1, n_back)
     slots = n_ep * group
     live = slots // 2
     dma = pltpu.SemaphoreType.DMA
@@ -284,7 +331,7 @@
             pltpu.VMEM((n_exp, group), jnp.int32),
             pltpu.VMEM((n_exp, group), F32),
             pltpu.VMEM((width, 2 * hidden), BF16),
-            pltpu.VMEM((chunks, hidden, n_tp * fc), BF16),
+            pltpu.VMEM((hidden, width), BF16),
             pltpu.VMEM((slots, n_tok), F32),
             pltpu.VMEM((n_tok, slots), BF16),
             pltpu.VMEM((n_tok, slots), BF16),
@@ -299,15 +346,18 @@
             pltpu.VMEM((live, hidden), BF16),
             pltpu.VMEM((chunks * n_tp, live, fc), BF16),
             pltpu.VMEM((chunks * n_tp, live, fc), BF16),
-            pltpu.VMEM((chunks, slots, fc), BF16),
-            pltpu.VMEM((chunks, slots, fc), BF16),
+            pltpu.VMEM((n_ret, slots, fc), BF16),
+            pltpu.VMEM((n_ret, slots, fc), BF16),
+            pltpu.VMEM((n_side, n_tok, fc), BF16),
+            pltpu.VMEM((n_side, n_tok, fc), BF16),
             dma((5,)),
             dma((2,)),
             dma((n_z,)),
             dma((chunks,)),
             dma((chunks,)),
-            dma((chunks,)),
-            dma((4,)),
+            dma((n_ret,)),
+            dma((n_side,)),
+            dma((5,)),
         ],
         compiler_params=pltpu.CompilerParams(collective_id=0, has_side_effects=True),
     )(tokens, selected, affinity, w_gate, w_up, w_down)

time: 30.6 us -> 29.3 us (0.958)
  Pallas kernels: 29.7 us -> 28.4 us
    pallas_call x1, Pallas kernels: 29.7 us -> 28.4 us  [per_device(): pl.pallas_call(functools.partial(kernel, n_ep, n_tp, chunks), out_shape=p...]
where the time goes in v3:
time: 29.3 us; the launch traced here: 29.1 us
  Pallas kernels  28.4 us (97%)
  local copies, waits for them, and re-layouts  0.66 us (2%)
    pallas_call x1, Pallas kernels, per_device(): pl.pallas_call(functools.partial(kernel, n_ep, n_tp, chunks), out_shape=p...  28.4 us
    unnamed x1, local copies, waits for them, and re-layouts  0.66 us

profile of v3, /device:TPU:0, one launch (start us, length us, event | category | flops | bytes accessed | tf_op | source)
XLA Modules:
  0.0 29.1 jit_solution(7437122452361691731)
XLA Ops:
  0.0 28.4 %shard_map.64 = bf16[128,512]{1,0:T(8,128)(2,1)S(1)} custom-call(bf16[128,2048]{1,0:T(8,128)(2,1)} %tok_hbm.1, s32[8,32]{1,0:T(8,128)} %sel_hbm.1, f32[8,32]{1,0:T(8,128)} %aff_hbm.1, bf16[1,2048,512]{2,1,0:T(8,128)(2,1)} %wg_hbm.1, bf16[1,2048,512]{2,1,0:T(8,128)(2,1)} %wu_hbm.1, bf16[1,512,2048]{2,1,0:T(8,128)(2,1)} %wd_hbm.1), custom_call_target="tpu_custom_call" | custom-call | tf_op jit(solution)/shard_map/pallas_call | solution.py:324
  28.4 0.7 %copy.8 = bf16[128,512]{1,0:T(8,128)(2,1)} copy(bf16[128,512]{1,0:T(8,128)(2,1)S(1)} %shard_map.64) | data formatting | bytes 262144

commit v4 on v3

--- a/solution.py
+++ b/solution.py
@@ -13,7 +13,7 @@
 BF16 = jnp.bfloat16
 CHUNK = 128
 OUT_EXTRA = 2
-RET_EXTRA = 2
+BACK = (0, 1)
 SIDE_AT = 2
 
 
@@ -31,7 +31,7 @@
     far = sorted(offsets, key=lambda o: -((o[0] > 0) + (o[1] > 0)))
     square = (height, width) == (2, 2)
     extra = list(range(chunks))[max(0, chunks - OUT_EXTRA):] if square and chunks > OUT_EXTRA else []
-    back = list(range(RET_EXTRA)) if square and chunks > RET_EXTRA else []
+    back = [c for c in BACK if square and chunks > max(BACK)]
     shared = [[o for o in far if not (c in extra and o == (1, 1))] for c in range(chunks)]
     reduced = [[o for o in far if not (c in back and o == (1, 1))] for c in range(chunks)]
     return width, height, far, extra, back, shared, reduced
@@ -46,7 +46,7 @@
     return order + [(c, (0, 0)) for c in range(chunks)]
 
 
-def kernel(
+def run(
     n_ep, n_tp, chunks,
     tok_hbm, sel_hbm, aff_hbm, wg_hbm, wu_hbm, wd_hbm, out_ref,
     tok, sel, aff, wgu, wd, onehot, weight_hi, weight_lo, expand, compact,
@@ -219,8 +219,9 @@
             send(
                 rows.at[at(c, tp)], rows.at[at(c, tp)],
                 s_out.at[1], s_x_r.at[c], {"tp": tp_to(o)})
-        if 0 < c <= len(extra):
-            spread_out(chunks + c - 1)
+        if c == 1:
+            for i in range(len(extra)):
+                spread_out(chunks + i)
         take(c, tp)
     for c in range(chunks):
         if c in extra:
@@ -289,8 +290,7 @@
     n_p = sum(len(offsets) for offsets in reduced)
     whole(part_in.at[pl.ds(0, n_p)], s_out.at[2], s_p_r.at[0]).wait_send()
 
-    plain = [c for c in range(chunks) if c not in back]
-    for c in plain[:1] + back + plain[1:]:
+    for c in [1, 0, *range(2, chunks)] if back else range(chunks):
         value = combined(c)
         if c in back:
             b = back.index(c)
@@ -301,6 +301,16 @@
     if back:
         whole(side_in, s_out.at[4], s_side_r.at[0]).wait_send()
     whole(ret_in.at[:, pl.ds(0, others), :], s_out.at[3], s_r_r.at[0]).wait_send()
+
+
+def kernel(n_ep, n_tp, chunks, *refs):
+    n_z = chunks + len(plan(n_tp, chunks)[3])
+    n_back = len(plan(n_tp, chunks)[4])
+    dma = pltpu.SemaphoreType.DMA
+    pl.run_scoped(
+        functools.partial(run, n_ep, n_tp, chunks, *refs),
+        dma((5,)), dma((2,)), dma((n_z,)), dma((chunks,)), dma((chunks,)), dma((chunks + n_back,)),
+        dma((max(1, n_back),)), dma((5,)))
 
 
 def per_device(tokens, selected, affinity, w_gate, w_up, w_down):
@@ -319,7 +329,6 @@
     n_side = max(1, n_back)
     slots = n_ep * group
     live = slots // 2
-    dma = pltpu.SemaphoreType.DMA
     any_spec = pl.BlockSpec(memory_space=pl.ANY)
     return pl.pallas_call(
         functools.partial(kernel, n_ep, n_tp, chunks),
@@ -350,14 +359,6 @@
             pltpu.VMEM((n_ret, slots, fc), BF16),
             pltpu.VMEM((n_side, n_tok, fc), BF16),
             pltpu.VMEM((n_side, n_tok, fc), BF16),
-            dma((5,)),
-            dma((2,)),
-            dma((n_z,)),
-            dma((chunks,)),
-            dma((chunks,)),
-            dma((n_ret,)),
-            dma((n_side,)),
-            dma((5,)),
         ],
         compiler_params=pltpu.CompilerParams(collective_id=0, has_side_effects=True),
     )(tokens, selected, affinity, w_gate, w_up, w_down)

time: 29.3 us -> 29 us (0.990)
  Pallas kernels: 28.4 us -> 28.1 us
    pallas_call x1, Pallas kernels: 28.4 us -> 28.1 us  [per_device(): pl.pallas_call(functools.partial(kernel, n_ep, n_tp, chunks), out_shape=p...]
where the time goes in v4:
time: 29 us; the launch traced here: 28.8 us
  Pallas kernels  28.1 us (97%)
  local copies, waits for them, and re-layouts  0.66 us (2%)
    pallas_call x1, Pallas kernels, per_device(): pl.pallas_call(functools.partial(kernel, n_ep, n_tp, chunks), out_shape=p...  28.1 us
    unnamed x1, local copies, waits for them, and re-layouts  0.66 us

profile of v4, /device:TPU:0, one launch (start us, length us, event | category | flops | bytes accessed | tf_op | source)
XLA Modules:
  0.0 28.8 jit_solution(4092413802999620976)
XLA Ops:
  0.0 28.1 %shard_map.64 = bf16[128,512]{1,0:T(8,128)(2,1)S(1)} custom-call(bf16[128,2048]{1,0:T(8,128)(2,1)} %refs_0_.1, s32[8,32]{1,0:T(8,128)} %refs_1_.1, f32[8,32]{1,0:T(8,128)} %refs_2_.1, bf16[1,2048,512]{2,1,0:T(8,128)(2,1)} %refs_3_.1, bf16[1,2048,512]{2,1,0:T(8,128)(2,1)} %refs_4_.1, bf16[1,512,2048]{2,1,0:T(8,128)(2,1)} %refs_5_.1), custom_call_target="tpu_custom_call" | custom-call | tf_op jit(solution)/shard_map/pallas_call | solution.py:333
  28.1 0.7 %copy.8 = bf16[128,512]{1,0:T(8,128)(2,1)} copy(bf16[128,512]{1,0:T(8,128)(2,1)S(1)} %shard_map.64) | data formatting | bytes 262144

commit v5 on v4

--- a/solution.py
+++ b/solution.py
@@ -12,7 +12,9 @@
 F32 = jnp.float32
 BF16 = jnp.bfloat16
 CHUNK = 128
-OUT_EXTRA = 2
+OUT_EXTRA = 1
+OUT_SPLIT = 2
+SPLIT_CORE = 0
 BACK = (0, 1)
 SIDE_AT = 2
 
@@ -30,11 +32,15 @@
     offsets = [(dy, dx) for dy in range(height) for dx in range(width)][1:]
     far = sorted(offsets, key=lambda o: -((o[0] > 0) + (o[1] > 0)))
     square = (height, width) == (2, 2)
-    extra = list(range(chunks))[max(0, chunks - OUT_EXTRA):] if square and chunks > OUT_EXTRA else []
+    both = chunks - OUT_EXTRA
+    some = both - OUT_SPLIT
+    extra = list(range(some, chunks)) if square and some > 0 else []
+    split = list(range(some, both)) if square and some > 0 else []
     back = [c for c in BACK if square and chunks > max(BACK)]
-    shared = [[o for o in far if not (c in extra and o == (1, 1))] for c in range(chunks)]
+    shared = [
+        [o for o in far if not (c in extra and c not in split and o == (1, 1))] for c in range(chunks)]
     reduced = [[o for o in far if not (c in back and o == (1, 1))] for c in range(chunks)]
-    return width, height, far, extra, back, shared, reduced
+    return width, height, far, extra, split, back, shared, reduced
 
 
 def pieces_of(far, back, reduced, chunks):
@@ -62,7 +68,9 @@
     feats = fc * chunks
     live = rows.shape[1]
     hidden = hid.shape[1]
-    width, height, far, extra, back, shared, reduced = plan(n_tp, chunks)
+    width, height, far, extra, split, back, shared, reduced = plan(n_tp, chunks)
+    over_ep = lax.rem(ep, 2) == SPLIT_CORE
+    over_tp = lax.rem(ep, 2) != SPLIT_CORE
     y, x = tp // width, lax.rem(tp, width)
 
     def tp_to(o):
@@ -154,6 +162,16 @@
 
     for d in ep_order:
         send(cnt_out.at[ep_to(d)], cnt_in.at[ep], s_cnt.at[0], s_cnt.at[1], {"ep": ep_to(d)})
+    def spread_some(i):
+        for j in range(n_ep // 2):
+            e = 2 * jnp.where(high_half > 0, j, n_ep // 2 - 1 - j) + SPLIT_CORE
+
+            @pl.when(e != ep)
+            def _(e=e):
+                send(
+                    z_out.at[i, rows_of(e), :], z_in.at[i, rows_of(ep), :],
+                    s_out.at[0], s_z_r.at[i], {"ep": e})
+
     def spread_out(i):
         for d in ep_order:
             send(
@@ -210,26 +228,50 @@
         rows[at(c, tp_to(o))] = jnp.dot(
             compact[...], z_in[i], preferred_element_type=F32).astype(BF16)
 
-    def arrive(c):
-        whole(rows.at[pl.ds(0, len(shared[c]))], s_out.at[1], s_x_r.at[c]).wait_recv()
+    def shared_in(c, n):
+        return whole(rows.at[pl.ds(0, n)], s_out.at[1], s_x_r.at[c])
 
     for c in range(chunks):
         squeeze(c)
         for o in shared[c]:
-            send(
-                rows.at[at(c, tp)], rows.at[at(c, tp)],
-                s_out.at[1], s_x_r.at[c], {"tp": tp_to(o)})
+            def share(c=c, o=o):
+                send(
+                    rows.at[at(c, tp)], rows.at[at(c, tp)],
+                    s_out.at[1], s_x_r.at[c], {"tp": tp_to(o)})
+
+            if c in split and o == (1, 1):
+                pl.when(over_tp)(share)
+            else:
+                share()
         if c == 1:
-            for i in range(len(extra)):
-                spread_out(chunks + i)
+            for i, b in enumerate(extra):
+                if b in split:
+                    spread_some(chunks + i)
+                else:
+                    spread_out(chunks + i)
         take(c, tp)
     for c in range(chunks):
-        if c in extra:
+        def direct(c=c):
             squeeze(chunks + extra.index(c))
             take(c, tp_to((1, 1)))
-        arrive(c)
+
+        if c in split:
+            @pl.when(over_ep)
+            def _(c=c):
+                direct()
+                shared_in(c, len(shared[c]) - 1).wait_recv()
+
+            @pl.when(over_tp)
+            def _(c=c):
+                shared_in(c, len(shared[c])).wait_recv()
+                take(c, tp_from((1, 1)))
+        else:
+            if c in extra:
+                direct()
+            shared_in(c, len(shared[c])).wait_recv()
         for o in shared[c]:
-            take(c, tp_from(o))
+            if not (c in split and o == (1, 1)):
+                take(c, tp_from(o))
 
     gate = acc[:, :hidden]
     up = acc[:, hidden:]
@@ -284,9 +326,25 @@
                     s_out.at[4], s_side_r.at[b], {"tp": tp_to((1, 1))})
 
     cnt_all.wait_send()
-    whole(z_in.at[:, pl.ds(0, others), :], s_out.at[0], s_z_r.at[0]).wait_send()
+    n_all = len(z_chunks) - len(split)
+    whole(z_in.at[pl.ds(0, n_all), pl.ds(0, others), :], s_out.at[0], s_z_r.at[0]).wait_send()
     n_x = sum(len(offsets) for offsets in shared)
-    whole(rows.at[pl.ds(0, n_x)], s_out.at[1], s_x_r.at[0]).wait_send()
+    if split:
+        def some_out(n):
+            return whole(
+                z_in.at[pl.ds(0, len(split)), pl.ds(0, n * group), :], s_out.at[0], s_z_r.at[0])
+
+        @pl.when(over_ep)
+        def _():
+            some_out(n_ep // 2 - 1).wait_send()
+            shared_in(0, n_x - len(split)).wait_send()
+
+        @pl.when(over_tp)
+        def _():
+            some_out(n_ep // 2).wait_send()
+            shared_in(0, n_x).wait_send()
+    else:
+        shared_in(0, n_x).wait_send()
     n_p = sum(len(offsets) for offsets in reduced)
     whole(part_in.at[pl.ds(0, n_p)], s_out.at[2], s_p_r.at[0]).wait_send()
 
@@ -305,7 +363,7 @@
 
 def kernel(n_ep, n_tp, chunks, *refs):
     n_z = chunks + len(plan(n_tp, chunks)[3])
-    n_back = len(plan(n_tp, chunks)[4])
+    n_back = len(plan(n_tp, chunks)[5])
     dma = pltpu.SemaphoreType.DMA
     pl.run_scoped(
         functools.partial(run, n_ep, n_tp, chunks, *refs),
@@ -324,7 +382,7 @@
     chunks = max(1, feats // CHUNK)
     fc = feats // chunks
     n_z = chunks + len(plan(n_tp, chunks)[3])
-    n_back = len(plan(n_tp, chunks)[4])
+    n_back = len(plan(n_tp, chunks)[5])
     n_ret = chunks + n_back
     n_side = max(1, n_back)
     slots = n_ep * group

time: 29 us -> 29 us (level)
  no operation moved by 1% of the time
where the time goes in v5:
time: 29 us; the launch traced here: 28.8 us
  Pallas kernels  28.1 us (97%)
  local copies, waits for them, and re-layouts  0.66 us (2%)
    pallas_call x1, Pallas kernels, per_device(): pl.pallas_call(functools.partial(kernel, n_ep, n_tp, chunks), out_shape=p...  28.1 us
    unnamed x1, local copies, waits for them, and re-layouts  0.66 us

profile of v5, /device:TPU:0, one launch (start us, length us, event | category | flops | bytes accessed | tf_op | source)
XLA Modules:
  0.0 28.8 jit_solution(13025971011413531734)
XLA Ops:
  0.0 28.1 %shard_map.64 = bf16[128,512]{1,0:T(8,128)(2,1)S(1)} custom-call(bf16[128,2048]{1,0:T(8,128)(2,1)} %refs_0_.1, s32[8,32]{1,0:T(8,128)} %refs_1_.1, f32[8,32]{1,0:T(8,128)} %refs_2_.1, bf16[1,2048,512]{2,1,0:T(8,128)(2,1)} %refs_3_.1, bf16[1,2048,512]{2,1,0:T(8,128)(2,1)} %refs_4_.1, bf16[1,512,2048]{2,1,0:T(8,128)(2,1)} %refs_5_.1), custom_call_target="tpu_custom_call" | custom-call | tf_op jit(solution)/shard_map/pallas_call | solution.py:391
  28.1 0.7 %copy.8 = bf16[128,512]{1,0:T(8,128)(2,1)} copy(bf16[128,512]{1,0:T(8,128)(2,1)S(1)} %shard_map.64) | data formatting | bytes 262144

commit v6 on v4

--- a/solution.py
+++ b/solution.py
@@ -161,9 +161,11 @@
                 s_out.at[0], s_z_r.at[i], {"ep": ep_to(d)})
 
     spread_out(0)
+    first = min(3, chunks)
     for i in range(1, chunks):
         gather(i)
-        spread_out(i)
+        if i < first:
+            spread_out(i)
 
     pltpu.make_async_copy(wg_hbm.at[0], wgu.at[:, pl.ds(0, hidden)], s_in.at[3]).start()
     pltpu.make_async_copy(wu_hbm.at[0], wgu.at[:, pl.ds(hidden, hidden)], s_in.at[3]).start()
@@ -219,6 +221,9 @@
             send(
                 rows.at[at(c, tp)], rows.at[at(c, tp)],
                 s_out.at[1], s_x_r.at[c], {"tp": tp_to(o)})
+        if c == 0:
+            for i in range(first, chunks):
+                spread_out(i)
         if c == 1:
             for i in range(len(extra)):
                 spread_out(chunks + i)

time: 29 us -> 28.7 us (0.990)
  Pallas kernels: 28.1 us -> 27.8 us
where the time goes in v6:
time: 28.7 us; the launch traced here: 28.5 us
  Pallas kernels  27.8 us (97%)
  local copies, waits for them, and re-layouts  0.66 us (2%)
    pallas_call x1, Pallas kernels, per_device(): pl.pallas_call(functools.partial(kernel, n_ep, n_tp, chunks), out_shape=p...  27.8 us
    unnamed x1, local copies, waits for them, and re-layouts  0.66 us

profile of v6, /device:TPU:0, one launch (start us, length us, event | category | flops | bytes accessed | tf_op | source)
XLA Modules:
  0.0 28.5 jit_solution(18289059091588996435)
XLA Ops:
  0.0 27.8 %shard_map.64 = bf16[128,512]{1,0:T(8,128)(2,1)S(1)} custom-call(bf16[128,2048]{1,0:T(8,128)(2,1)} %refs_0_.1, s32[8,32]{1,0:T(8,128)} %refs_1_.1, f32[8,32]{1,0:T(8,128)} %refs_2_.1, bf16[1,2048,512]{2,1,0:T(8,128)(2,1)} %refs_3_.1, bf16[1,2048,512]{2,1,0:T(8,128)(2,1)} %refs_4_.1, bf16[1,512,2048]{2,1,0:T(8,128)(2,1)} %refs_5_.1), custom_call_target="tpu_custom_call" | custom-call | tf_op jit(solution)/shard_map/pallas_call | solution.py:338
  27.8 0.7 %copy.8 = bf16[128,512]{1,0:T(8,128)(2,1)} copy(bf16[128,512]{1,0:T(8,128)(2,1)S(1)} %shard_map.64) | data formatting | bytes 262144

commit v7 on v6

--- a/solution.py
+++ b/solution.py
@@ -40,9 +40,7 @@
 def pieces_of(far, back, reduced, chunks):
     order = []
     for c in range(chunks):
-        order += [(c, o) for o in reduced[c]]
-        if c == 0:
-            order += [(b, (1, 1)) for b in back]
+        order += [(c, (1, 1))] * (c in back) + [(c, o) for o in reduced[c]]
     return order + [(c, (0, 0)) for c in range(chunks)]
 
 

time: 28.7 us -> 28.7 us (level)
  no operation moved by 1% of the time
where the time goes in v7:
time: 28.7 us; the launch traced here: 28.5 us
  Pallas kernels  27.8 us (97%)
  local copies, waits for them, and re-layouts  0.66 us (2%)
    pallas_call x1, Pallas kernels, per_device(): pl.pallas_call(functools.partial(kernel, n_ep, n_tp, chunks), out_shape=p...  27.8 us
    unnamed x1, local copies, waits for them, and re-layouts  0.66 us

profile of v7, /device:TPU:0, one launch (start us, length us, event | category | flops | bytes accessed | tf_op | source)
XLA Modules:
  0.0 28.5 jit_solution(15127374231897088296)
XLA Ops:
  0.0 27.8 %shard_map.64 = bf16[128,512]{1,0:T(8,128)(2,1)S(1)} custom-call(bf16[128,2048]{1,0:T(8,128)(2,1)} %refs_0_.1, s32[8,32]{1,0:T(8,128)} %refs_1_.1, f32[8,32]{1,0:T(8,128)} %refs_2_.1, bf16[1,2048,512]{2,1,0:T(8,128)(2,1)} %refs_3_.1, bf16[1,2048,512]{2,1,0:T(8,128)(2,1)} %refs_4_.1, bf16[1,512,2048]{2,1,0:T(8,128)(2,1)} %refs_5_.1), custom_call_target="tpu_custom_call" | custom-call | tf_op jit(solution)/shard_map/pallas_call | solution.py:336
  27.9 0.7 %copy.8 = bf16[128,512]{1,0:T(8,128)(2,1)} copy(bf16[128,512]{1,0:T(8,128)(2,1)S(1)} %shard_map.64) | data formatting | bytes 262144
